TPU v7x, 512 devices: a 8x2x16 block of a 8x16x16 slice. The times are simulated.
512 devices in a mesh: grp: 2 (over y), ep: 16 (over z), tp: 16 (over x, core).
Axes of the slice: x: 8, y: 2, z: 16, core: 2. Of those that a mesh axis runs over, the one named last changes fastest.
The devices are a block of a 8x16x16 slice.
Arguments:
- queries: bfloat16 [65536, 1024], P(('grp', 'ep'), 'tp'), parts along dimension 0, may hold values from -6 to 6
- key_vectors: bfloat16 [65536, 1024], P(('grp', 'ep'), 'tp'), parts along dimension 0, may hold values from -6 to 6
- value_vectors: bfloat16 [65536, 1024], P(('grp', 'ep'), 'tp'), parts along dimension 0, may hold values from -6 to 6
- input_gate: float32 [65536, 16], P(('grp', 'ep'), 'tp'), parts along dimension 0, may hold values from -6 to 320
- forget_gate: float32 [65536, 16], P(('grp', 'ep'), 'tp'), parts along dimension 0, may hold values from 0 to 15
- head_gain: float32 [1024], P('tp'), may hold values from 0.1 to 1.9
- out_weight: bfloat16 [1024, 2048], P(None, 'tp'), may hold values from -0.1875 to 0.1875
- expert_input: bfloat16 [4096, 2048], P(('grp', 'ep')), parts along dimension 0, may hold values from -6 to 6
- norm_gain: float32 [2048], replicated, may hold values from 0.1 to 1.9
- routes: int32 [4096, 2], P(('grp', 'ep')), parts along dimension 0, may hold values from 0 to 15, all different within a row; in each aligned block of 128 rows (0 to 127, 128 to 255, ...) at most 20 rows name the same one
- route_weight: float32 [4096, 2], P(('grp', 'ep')), parts along dimension 0, may hold values from 0.25 to 1
- gate_weight: bfloat16 [16, 2048, 3584], P('ep', None, 'tp'), may hold values from -0.125 to 0.125
- up_weight: bfloat16 [16, 2048, 3584], P('ep', None, 'tp'), may hold values from -0.125 to 0.125
- down_weight: bfloat16 [16, 3584, 2048], P('ep', 'tp'), may hold values from -0.125 to 0.125
Outputs:
- mixer_out: bfloat16 [65536, 2048], P(('grp', 'ep'), 'tp'), parts along dimension 0
- expert_out: bfloat16 [4096, 2048], P(('grp', 'ep'), 'tp'), parts along dimension 0
There are 2 independent parts, one for each index of `grp`. A program takes and returns all parts, laid end to end along the dimension named above; an argument that names none is the same for every part. Nothing has to cross between parts.
Inputs may be any that keep to these rules, and one draw needn't show every extreme that they name: `routes`: A token's 2 experts differ. Among the 128 tokens of one index of ep, no expert is named more than 20 times, and in some of these blocks one is named exactly 20 times.
All inputs are finite; a program needn't handle non-finite values.
Results may differ from a plain program's by a relative error of at most 0.019.
Values may be sent and summed in bfloat16 or wider, within the bound.
No kernel may reach another device: no remote copies, remote signals or barrier semaphores. Data moves between devices by JAX's collectives and lax.ppermute only.
A program may use at most 64 MiB of HBM per device.

v0:
```python
import jax
import jax.numpy as jnp
from jax import lax
from jax.sharding import Mesh
from jax.sharding import PartitionSpec as P

HEAD = 64
BLK = 128
TP = ("tp_0", "tp_1")


EXACT_PRECISION = lax.Precision.HIGHEST
VERY_NEGATIVE = -1e30


def copy_for_each(shard, axis):
    peers = lax.axis_size(axis)
    return lax.all_to_all(
        jnp.broadcast_to(shard[None], (peers, *shard.shape)), axis, 0, 0, tiled=True
    )


def all_in_one(shard, axis):
    leaves = jax.tree.leaves(shard)
    sequence = sorted(range(len(leaves)), key=lambda k: -leaves[k].size)
    width = (1, *leaves[sequence[0]].shape)[-1]
    lines = [
        jnp.pad(leaves[k].reshape(-1), (0, -leaves[k].size % width)).reshape(-1, width)
        for k in sequence
    ]
    both, at, found = (copy_for_each(jnp.concatenate(lines), axis), 0, {})
    for k, line in zip(sequence, lines):
        section = both[:, at : at + len(line)].reshape(len(both), -1)
        found[k] = section[:, : leaves[k].size].reshape(-1, *leaves[k].shape)
        at += len(line)
    numbers = iter(range(len(leaves)))
    return jax.tree.map(lambda _: found[next(numbers)], shard)


def joined_by_halves(pieces, combine):
    while len(jax.tree.leaves(pieces)[0]) > 1:
        pieces = jax.vmap(combine)(
            *(jax.tree.map(lambda part: part[side::2], pieces) for side in (0, 1))
        )
    return jax.tree.map(lambda part: part[0], pieces)


def prefix(shard, axis, combine, identity):
    peers, index = (lax.axis_size(axis), lax.axis_index(axis))
    passed = jnp.arange(peers) < index

    def kept(part, zero, own):
        part = jnp.where(
            passed.reshape(-1, *(1 for _ in own.shape)), part, jnp.asarray(zero, own.dtype)
        )
        return part

    pieces = all_in_one(shard, axis)
    return joined_by_halves(jax.tree.map(kept, pieces, identity, shard), combine)


def gathered_by_axis(shard, axes, dim):
    for axis in reversed(axes):
        shard = lax.all_gather(shard, axis, axis=dim, tiled=True)
    return shard


def split_up(shard, dim, peers):
    lengths = shard.shape
    parts = shard.reshape(*lengths[:dim], peers, lengths[dim] // peers, *lengths[dim + 1 :])
    return jnp.moveaxis(parts, dim, 0)


def sent_and_summed(shard, axis, dim):
    parts = split_up(shard, dim, lax.axis_size(axis))
    arrived = lax.all_to_all(parts, axis, split_axis=0, concat_axis=0, tiled=True)
    return arrived.astype(jnp.float32).sum(axis=0)


def combine_states(before_part, after_part):
    decay_early, matrix_early, normer_early, stable_early = before_part
    decay_late, matrix_late, normer_late, stable_late = after_part
    highest = jnp.maximum(decay_late + stable_early, stable_late)
    scale_early = jnp.exp(decay_late + stable_early - highest)
    scale_late = jnp.exp(stable_late - highest)
    matrix_joined = (
        scale_early[..., None, None] * matrix_early + scale_late[..., None, None] * matrix_late
    )
    normer_joined = scale_early[..., None] * normer_early + scale_late[..., None] * normer_late
    return (decay_early + decay_late, matrix_joined, normer_joined, highest)


def memory_cells(queries, key_vectors, value_vectors, input_gate, forget_gate, head_gain):
    segment_len = input_gate.shape[0]
    heads = input_gate.shape[1]
    blocks = segment_len // BLK
    head_scale = HEAD ** (-0.5)

    def block_view(matrix):
        return matrix.reshape(blocks, BLK, heads, HEAD).transpose(2, 0, 1, 3)

    query_blocks = block_view(queries)
    key_blocks = block_view(key_vectors)
    value_blocks = block_view(value_vectors)
    input_blocks = input_gate.reshape(blocks, BLK, heads).transpose(2, 0, 1)
    log_forget = jax.nn.log_sigmoid(forget_gate).reshape(blocks, BLK, heads).transpose(2, 0, 1)
    running_decay = jnp.cumsum(log_forget, axis=-1)
    block_end = running_decay[..., -1]
    tail_gate = block_end[..., None] - running_decay + input_blocks
    block_peak = jnp.max(tail_gate, axis=-1)
    key_weight = jnp.exp(tail_gate - block_peak[..., None])
    key_weighted_rows = (key_weight[..., None] * key_blocks).astype(jnp.bfloat16)
    matrix_terms = jnp.einsum(
        "hcsk,hcsv->hckv", key_weighted_rows, value_blocks, preferred_element_type=jnp.float32
    )
    normer_terms = jnp.sum(key_weighted_rows.astype(jnp.float32), axis=2)
    inclusive = lax.associative_scan(
        combine_states, (block_end, matrix_terms, normer_terms, block_peak), axis=1
    )
    device_total = tuple((member[:, -1] for member in inclusive))
    identity = (
        jnp.zeros((heads,), jnp.float32),
        jnp.zeros((heads, HEAD, HEAD), jnp.float32),
        jnp.zeros((heads, HEAD), jnp.float32),
        jnp.full((heads,), VERY_NEGATIVE, jnp.float32),
    )
    earlier_states = prefix(device_total, "ep", combine_states, identity)
    initial = (
        jnp.zeros((heads,), jnp.float32),
        jnp.zeros((heads, HEAD, HEAD), jnp.float32),
        jnp.zeros((heads, HEAD), jnp.float32),
        jnp.zeros((heads,), jnp.float32),
    )
    entering = combine_states(initial, earlier_states)
    local_entry = tuple(
        (
            jnp.concatenate([start_value[:, None], member[:, :-1]], axis=1)
            for start_value, member in zip(identity, inclusive)
        )
    )
    incoming = tuple((member[:, None] for member in entering))
    ignored, matrix_entry, normer_entry, stable_entry = combine_states(incoming, local_entry)
    causal = jnp.arange(BLK)[:, None] >= jnp.arange(BLK)[None, :]
    log_weights = (
        running_decay[..., :, None] - running_decay[..., None, :] + input_blocks[..., None, :]
    )
    log_weights = jnp.where(causal, log_weights, -jnp.inf)
    stabilizer = jnp.maximum(running_decay + stable_entry[..., None], jnp.max(log_weights, axis=-1))
    scores = (
        jnp.einsum("hcjd,hcsd->hcjs", query_blocks, key_blocks, preferred_element_type=jnp.float32)
        * head_scale
    )
    weighted = jnp.exp(log_weights - stabilizer[..., None]) * scores
    carried_scale = jnp.exp(running_decay + stable_entry[..., None] - stabilizer)
    query_wide = query_blocks.astype(jnp.float32)
    carried = (
        jnp.einsum("hcjk,hckv->hcjv", query_wide, matrix_entry, precision=EXACT_PRECISION)
        * head_scale
    )
    numerator = carried_scale[..., None] * carried + jnp.einsum(
        "hcjs,hcsv->hcjv",
        weighted.astype(jnp.bfloat16),
        value_blocks,
        preferred_element_type=jnp.float32,
    )
    denominator = carried_scale * jnp.einsum(
        "hcjk,hck->hcj", query_wide, normer_entry, precision=EXACT_PRECISION
    ) * head_scale + jnp.sum(weighted, axis=-1)
    cells = numerator / jnp.maximum(jnp.abs(denominator), jnp.exp(-stabilizer))[..., None]
    normed = cells * lax.rsqrt(jnp.mean(cells * cells, axis=-1, keepdims=True) + 1e-06)
    normed = (normed * head_gain.reshape(heads, 1, 1, HEAD)).astype(jnp.bfloat16)
    return normed.transpose(1, 2, 0, 3).reshape(segment_len, heads * HEAD)


def on_device(
    queries,
    key_vectors,
    value_vectors,
    input_gate,
    forget_gate,
    head_gain,
    out_weight,
    expert_input,
    norm_gain,
    routes,
    route_weight,
    gate_weight,
    up_weight,
    down_weight,
):
    normed = memory_cells(queries, key_vectors, value_vectors, input_gate, forget_gate, head_gain)
    mixer_out = jnp.dot(
        lax.all_gather(normed, TP, axis=1, tiled=True),
        out_weight,
        preferred_element_type=jnp.float32,
    ).astype(jnp.bfloat16)
    tokens = expert_input.shape[0]
    row_width = expert_input.shape[1]
    choices_per = routes.shape[1]
    experts = lax.axis_size("ep")
    splits = lax.axis_size(TP)
    slice_width = row_width // splits
    capacity = 5 * tokens * choices_per // (4 * experts)
    input_wide = expert_input.astype(jnp.float32)
    scaled = input_wide * lax.rsqrt(
        jnp.mean(input_wide * input_wide, axis=-1, keepdims=True) + 1e-06
    )
    scaled = scaled * norm_gain
    chosen = routes.reshape(-1)
    onehot = (chosen[:, None] == jnp.arange(experts, dtype=jnp.int32)[None, :]).astype(jnp.int32)
    slot_index = jnp.sum((jnp.cumsum(onehot, axis=0) - onehot) * onehot, axis=1)
    target = chosen * capacity + slot_index
    source = jnp.repeat(jnp.arange(tokens, dtype=jnp.int32), choices_per)
    column_start = lax.axis_index(TP) * slice_width
    narrow = lax.dynamic_slice_in_dim(scaled, column_start, slice_width, 1).astype(jnp.bfloat16)
    outgoing = (
        jnp.zeros((experts * capacity, slice_width), jnp.bfloat16).at[target].set(narrow[source])
    )
    arrived = lax.all_to_all(
        outgoing.reshape(experts, capacity, slice_width),
        "ep",
        split_axis=0,
        concat_axis=0,
        tiled=True,
    )
    portion = gathered_by_axis(arrived, TP, 2)
    flat_rows = portion.reshape(experts * capacity, portion.shape[2])
    gate_rows = gate_weight[0]
    up_rows = up_weight[0]
    gate_act = jnp.dot(flat_rows, gate_rows, preferred_element_type=jnp.float32)
    up_act = jnp.dot(flat_rows, up_rows, preferred_element_type=jnp.float32)
    hidden = (jax.nn.silu(gate_act) * up_act).astype(jnp.bfloat16)
    piece_sum = jnp.dot(hidden, down_weight[0], preferred_element_type=jnp.float32).astype(
        jnp.bfloat16
    )
    summed = sent_and_summed(piece_sum, TP, 1).astype(jnp.bfloat16)
    returned = lax.all_to_all(
        summed.reshape(experts, capacity, slice_width),
        "ep",
        split_axis=0,
        concat_axis=0,
        tiled=True,
    )
    returned = returned.reshape(experts * capacity, slice_width)
    copies = returned[target].astype(jnp.float32).reshape(tokens, choices_per, slice_width)
    expert_out = jnp.sum(copies * route_weight[..., None], axis=1).astype(jnp.bfloat16)
    return (mixer_out, expert_out)


def solution(mesh):
    torus = Mesh(
        mesh.devices.reshape(mesh.shape["grp"], mesh.shape["ep"], 8, 2),
        ("grp", "ep", "tp_0", "tp_1"),
    )
    in_specs = (
        P(("grp", "ep"), TP),
        P(("grp", "ep"), TP),
        P(("grp", "ep"), TP),
        P(("grp", "ep"), TP),
        P(("grp", "ep"), TP),
        P(TP),
        P(None, TP),
        P(("grp", "ep"), None),
        P(),
        P(("grp", "ep"), None),
        P(("grp", "ep"), None),
        P("ep", None, TP),
        P("ep", None, TP),
        P("ep", TP, None),
    )
    out_specs = (P(("grp", "ep"), TP), P(("grp", "ep"), TP))
    return jax.shard_map(
        on_device, mesh=torus, in_specs=in_specs, out_specs=out_specs, check_vma=False
    )
```

profile of v0, /device:TPU:65, one launch (start us, length us, event | category | flops | bytes accessed | tf_op | source)
XLA Modules:
  0.0 246.1 jit_solution(6144503477098120845)
XLA Ops:
  7.2 1.2 convert_element_type.101
  8.5 0.2 multiply_reduce_fusion
  9.1 0.6 reduce-window.6
  9.7 0.2 slice_reduce_fusion
  10.4 0.8 dynamic-slice
  11.3 1.8 scatter_custom_fusion
  13.1 0.7 reshape.885
  13.8 44.2 %all-to-all-start.1 = ((bf16[16,20,128]{2,1,0:T(8,128)(2,1)}), bf16[16,20,128]{2,1,0:T(8,128)(2,1)S(1)}, u32[]{:S(2)}, u32[]{:S(2)}) async-start(bf16[16,20,128]{2,1,0:T(8,128)(2,1)} %reshape.885), calls=%async_computation.1 | async-start | bytes 196608 | tf_op jit(solution)/shard_map/all_to_all | solution.py:219
  58.1 0.3 reduce_window_sum.28
  58.4 0.2 slice_reduce_fusion.1
  58.8 0.2 add_reduce_fusion
  60.0 0.6 fusion.92
  63.1 0.7 pad_add_fusion.2
  63.8 0.6 fusion.91
  64.5 0.6 fusion.93
  67.7 0.2 convert_reduce_fusion
  68.2 0.3 copy-done.6
  68.5 0.3 convolution_bitcast_fusion
  71.7 0.8 pad_add_fusion.3
  73.2 0.7 pad_maximum_fusion.7
  74.0 0.7 pad_maximum_fusion.10
  77.2 0.7 slice.446
  77.9 0.7 pad_bitcast_fusion.1
  78.8 0.7 slice.448
  79.6 0.7 pad_bitcast_fusion
  80.7 0.7 select_reduce_fusion
  81.4 0.8 broadcast_in_dim.39
  82.2 11.5 %all-to-all-start = ((f32[16,67,64]{1,2,0:T(8,128)}), f32[16,67,64]{1,2,0:T(8,128)S(1)}, u32[]{:S(2)}, u32[]{:S(2)}) async-start(f32[16,67,64]{1,2,0:T(8,128)} %broadcast_in_dim.39), calls=%async_computation | async-start | bytes 1048576 | tf_op jit(solution)/shard_map/all_to_all | solution.py:18
  93.7 0.5 iota_compare_fusion.4
  94.5 0.5 slice_bitcast_fusion.1
  95.0 0.6 slice_bitcast_fusion
  95.7 3.3 %all_gather.10 = bf16[16,20,256]{2,1,0:T(8,128)(2,1)} all-gather(bf16[16,20,128]{2,1,0:T(8,128)(2,1)S(1)} %all-to-all-done.1), channel_id=1, replica_groups=mesh['grp'=2,'ep'=16,'tp_0'=8,'tp_1'=2] {'tp_1'}, dimensions={2}, use_global_device_ids=true | all-gather | bytes 245760 | tf_op jit(solution)/shard_map/all_gather | solution.py:64
  99.0 0.2 all-gather.3.cloned.1.call-start
  99.3 17.3 %all-to-all-done = f32[16,67,64]{1,2,0:T(8,128)S(1)} async-done(((f32[16,67,64]{1,2,0:T(8,128)}), f32[16,67,64]{1,2,0:T(8,128)S(1)}, u32[]{:S(2)}, u32[]{:S(2)}) %all-to-all-start) | async-done | bytes 274464 | tf_op jit(solution)/shard_map/all_to_all | solution.py:18
  116.5 1.1 slice_select_fusion
  117.6 0.8 copy.142
  118.4 1.3 slice_select_fusion.3
  119.8 1.3 slice.451
  121.1 1.3 slice.452
  122.4 0.8 copy.143
  123.2 0.7 slice_select_fusion.2
  124.0 0.7 fusion.86
  125.3 0.6 fusion.88
  125.9 0.6 fusion.90
  130.4 0.8 subtract_exponential_fusion.3
  131.1 0.8 subtract_exponential_fusion.2
  132.5 0.3 fusion.26
  132.9 0.9 fusion.98
  134.3 0.5 fusion.3
  135.0 0.3 multiply_reduce_fusion.1
  135.3 0.4 copy-done.18
  135.6 0.8 copy_bitcast_fusion
  136.5 9.5 %all-gather.5.cloned.1.call-done = bf16[16,20,2048]{2,1,0:T(8,128)(2,1)} async-done(((bf16[16,20,256]{2,1,0:T(8,128)(2,1)}), bf16[16,20,2048]{2,1,0:T(8,128)(2,1)}) %all-gather.5.cloned.1.call-update) | async-done | bytes 1310736 | tf_op jit(solution)/shard_map/all_gather | solution.py:64
  146.0 2.3 reshape.886
  148.3 1.3 fusion.7
  149.6 2.8 %fusion = bf16[40,16,8,128]{3,2,1,0:T(8,128)(2,1)S(1)} fusion(bf16[1,224,2048]{2,1,0:T(8,128)(2,1)S(1)} %copy-done, bf16[320,2048]{1,0:T(8,128)(2,1)S(1)} %reshape.886, bf16[1,2048,224]{1,2,0:T(8,128)(2,1)} %param.26, f32[320,224]{1,0:T(8,128)} %fusion.7), kind=kOutput, calls=%fused_computation.5 | convolution fusion | flops 588288000 | bytes 4743168 | tf_op jit(solution)/shard_map/dot_general | solution.py:233
  152.4 0.3 copy.188
  152.7 54.8 %all_to_all.20 = bf16[16,320,128]{2,1,0:T(8,128)(2,1)S(1)} all-to-all(bf16[16,320,128]{2,1,0:T(8,128)(2,1)S(1)} %bitcast.198), channel_id=1, replica_groups=mesh['grp'=2,'ep'=16,'tp_0'=8,'tp_1'=2] {'tp_0','tp_1'}, dimensions={0} | all-to-all | bytes 2621440 | tf_op jit(solution)/shard_map/all_to_all | solution.py:76
  207.7 0.7 reshape.888
  208.4 12.7 %all-to-all-start.3 = ((bf16[16,20,128]{2,1,0:T(8,128)(2,1)}), bf16[16,20,128]{2,1,0:T(8,128)(2,1)S(1)}, u32[]{:S(2)}, u32[]{:S(2)}) async-start(bf16[16,20,128]{2,1,0:T(8,128)(2,1)} %reshape.888), calls=%async_computation.3 | async-start | bytes 196608 | tf_op jit(solution)/shard_map/all_to_all | solution.py:237
  221.3 11.9 %all-to-all-done.3 = bf16[16,20,128]{2,1,0:T(8,128)(2,1)S(1)} async-done(((bf16[16,20,128]{2,1,0:T(8,128)(2,1)}), bf16[16,20,128]{2,1,0:T(8,128)(2,1)S(1)}, u32[]{:S(2)}, u32[]{:S(2)}) %all-to-all-start.3) | async-done | bytes 81952 | tf_op jit(solution)/shard_map/all_to_all | solution.py:237
  233.2 0.9 gather_fusion
  234.0 0.9 fusion.46
  234.9 4.3 %convolution_convert_fusion.1 = bf16[2048,128]{1,0:T(8,128)(2,1)} fusion(bf16[2048,1024]{0,1:T(8,128)(2,1)} %all-gather.3.cloned.1.call-done, bf16[1024,128]{1,0:T(8,128)(2,1)S(1)} %copy-done.19), kind=kOutput, calls=%fused_computation.4 | convolution fusion | flops 537133056 | bytes 4980736 | tf_op jit(solution)/shard_map/dot_general | solution.py:192
  (208 shorter events, 10.6 us)
Async XLA Ops:
  7.2 142.4 %copy-start = (bf16[1,224,2048]{2,1,0:T(8,128)(2,1)S(1)}, bf16[1,224,2048]{2,1,0:T(8,128)(2,1)}, u32[]{:S(2)}) copy-start(bf16[1,224,2048]{2,1,0:T(8,128)(2,1)} %param.27) | copy-start | bytes 2752516
  7.2 1.3 copy-start.1
  7.2 1.5 copy-start.13
  7.2 50.8 %copy-start.12 = (f32[2048,1]{0,1:T(1,128)S(1)}, f32[2048,1]{0,1:T(1,128)}, u32[]{:S(2)}) copy-start(f32[2048,1]{0,1:T(1,128)} %param.18) | copy-start | bytes 24580
  7.2 51.5 %copy-start.8 = (f32[2048,1]{0,1:T(1,128)S(1)}, f32[2048,1]{0,1:T(1,128)}, u32[]{:S(2)}) copy-start(f32[2048,1]{0,1:T(1,128)} %param.17) | copy-start | bytes 24580
  8.5 59.0 %copy-start.2 = (bf16[2048,64]{0,1:T(8,128)(2,1)S(1)}, bf16[2048,64]{0,1:T(8,128)(2,1)}, u32[]{:S(2)}) copy-start(bf16[2048,64]{0,1:T(8,128)(2,1)} %param.15) | copy-start | bytes 786436
  11.3 2.5 %copy-start.14 = (s32[256,1]{0,1:T(1,128)}, s32[256,1]{0,1:T(1,128)S(1)}, u32[]{:S(2)}) copy-start(s32[256,1]{0,1:T(1,128)S(1)} %compare_select_fusion.2) | copy-start | bytes 3076
  13.8 67.5 %all-to-all-start.1 = ((bf16[16,20,128]{2,1,0:T(8,128)(2,1)}), bf16[16,20,128]{2,1,0:T(8,128)(2,1)S(1)}, u32[]{:S(2)}, u32[]{:S(2)}) async-start(bf16[16,20,128]{2,1,0:T(8,128)(2,1)} %reshape.885), calls=%async_computation.1 | async-start | bytes 196608 | tf_op jit(solution)/shard_map/all_to_all | solution.py:219
  67.6 1.0 copy-start.6
  70.3 10.2 %copy-start.10 = (pred[128,128]{0,1:T(8,128)(4,1)}, pred[128,128]{0,1:T(8,128)(4,1)S(1)}, u32[]{:S(2)}) copy-start(pred[128,128]{0,1:T(8,128)(4,1)S(1)} %iota_compare_fusion) | copy-start | bytes 49156
  82.2 34.3 %all-to-all-start = ((f32[16,67,64]{1,2,0:T(8,128)}), f32[16,67,64]{1,2,0:T(8,128)S(1)}, u32[]{:S(2)}, u32[]{:S(2)}) async-start(f32[16,67,64]{1,2,0:T(8,128)} %broadcast_in_dim.39), calls=%async_computation | async-start | bytes 1048576 | tf_op jit(solution)/shard_map/all_to_all | solution.py:18
  93.7 52.4 %all-gather.5.cloned.1.call-start = ((), (), s32[]{:S(2)}) async-start(), calls=%async_computation.5 | async-start | bytes 1769472 | tf_op jit(solution)/shard_map/all_gather | solution.py:64
  99.0 135.9 %all-gather.3.cloned.1.call-start = ((), (), s32[]{:S(2)}) async-start(), calls=%async_computation.4 | async-start | bytes 4456448 | tf_op jit(solution)/shard_map/all_gather | solution.py:193
  118.4 14.1 %copy-start.5 = (bf16[2048,64]{0,1:T(8,128)(2,1)S(1)}, bf16[2048,64]{0,1:T(8,128)(2,1)}, u32[]{:S(2)}) copy-start(bf16[2048,64]{0,1:T(8,128)(2,1)} %param.14) | copy-start | bytes 786436
  119.8 13.1 %copy-start.3 = (bf16[2048,64]{0,1:T(8,128)(2,1)S(1)}, bf16[2048,64]{0,1:T(8,128)(2,1)}, u32[]{:S(2)}) copy-start(bf16[2048,64]{0,1:T(8,128)(2,1)} %param.15) | copy-start | bytes 786436
  123.2 9.6 %copy-start.9 = (f32[2048,1]{0,1:T(1,128)S(1)}, f32[2048,1]{0,1:T(1,128)}, u32[]{:S(2)}) copy-start(f32[2048,1]{0,1:T(1,128)} %param.17) | copy-start | bytes 24580
  123.2 9.6 %copy-start.11 = (pred[128,128]{0,1:T(8,128)(4,1)S(1)}, pred[128,128]{0,1:T(8,128)(4,1)}, u32[]{:S(2)}) copy-start(pred[128,128]{0,1:T(8,128)(4,1)} %copy-done.10) | copy-start | bytes 49156
  132.9 1.0 copy-start.16
  134.0 1.0 copy-start.7
  135.0 0.7 copy-start.18
  136.5 11.8 %copy-start.4 = (bf16[1,2048,224]{1,2,0:T(8,128)(2,1)S(1)}, bf16[1,2048,224]{1,2,0:T(8,128)(2,1)}, u32[]{:S(2)}) copy-start(bf16[1,2048,224]{1,2,0:T(8,128)(2,1)} %param.25) | copy-start | bytes 2752516
  207.5 13.6 %copy-start.17 = (f32[128,2]{0,1:T(2,128)S(1)}, f32[128,2]{0,1:T(2,128)}, u32[]{:S(2)}) copy-start(f32[128,2]{0,1:T(2,128)} %param.24) | copy-start | bytes 3076
  207.5 13.7 %copy-start.15 = (s32[256,1]{0,1:T(1,128)S(1)}, s32[256,1]{0,1:T(1,128)}, u32[]{:S(2)}) copy-start(s32[256,1]{0,1:T(1,128)} %copy-done.14) | copy-start | bytes 3076
  207.5 27.4 %copy-start.19 = (bf16[1024,128]{1,0:T(8,128)(2,1)S(1)}, bf16[1024,128]{1,0:T(8,128)(2,1)}, u32[]{:S(2)}) copy-start(bf16[1024,128]{1,0:T(8,128)(2,1)} %param.20) | copy-start | bytes 786436
  208.4 24.8 %all-to-all-start.3 = ((bf16[16,20,128]{2,1,0:T(8,128)(2,1)}), bf16[16,20,128]{2,1,0:T(8,128)(2,1)S(1)}, u32[]{:S(2)}, u32[]{:S(2)}) async-start(bf16[16,20,128]{2,1,0:T(8,128)(2,1)} %reshape.888), calls=%async_computation.3 | async-start | bytes 196608 | tf_op jit(solution)/shard_map/all_to_all | solution.py:237
Sparse Core Ops, SparseCore 0:
  99.2 46.8 all-gather.4
  148.2 70.7 all-gather.2
where the time goes:
time: 247 us; the launch traced here: 246 us
  starting transfers between devices  68.7 us (28%)
  blocking collectives  58.1 us (24%)
  waiting for transfers between devices  38.8 us (16%)
  local copies, waits for them, and re-layouts  26.6 us (11%)
  between operations  25.4 us (10%)
  other arithmetic  17.8 us (7%)
  matrix products  10.7 us (4%)
    all_to_all x1, blocking collectives, sent_and_summed(): lax.all_to_all(parts, axis, split_axis=0, concat_axis=0, tiled=True)  54.8 us
    all_to_all x1, starting transfers between devices, on_device(): lax.all_to_all(outgoing.reshape(experts, capacity, slice_width), 'ep', sp...  44.2 us
    all_to_all x1, waiting for transfers between devices, copy_for_each(): lax.all_to_all(jnp.broadcast_to(shard[None], (peers, *shard.shape)), axis...  17.3 us
    all_to_all x1, starting transfers between devices, on_device(): lax.all_to_all(summed.reshape(experts, capacity, slice_width), 'ep', spli...  12.7 us
    all_to_all x1, waiting for transfers between devices, on_device(): lax.all_to_all(summed.reshape(experts, capacity, slice_width), 'ep', spli...  11.9 us
    all_to_all x1, starting transfers between devices, copy_for_each(): lax.all_to_all(jnp.broadcast_to(shard[None], (peers, *shard.shape)), axis...  11.5 us
    all_gather x1, waiting for transfers between devices, gathered_by_axis(): shard = lax.all_gather(shard, axis, axis=dim, tiled=True)  9.52 us
  transfers between devices with their start and end apart: 5, of which 3 were waited for; matrix products, arithmetic and copies ran while one was open for 17% of the time, Pallas kernels for 0%

commit v1 on v0

v1 whole, which is shorter than its diff:
```python
import functools

import jax
import jax.numpy as jnp
from jax import lax
from jax.experimental import pallas as pl
from jax.experimental.pallas import tpu as pltpu
from jax.sharding import Mesh
from jax.sharding import PartitionSpec as P

HEAD = 64
BLK = 128
TP = ("tp_0", "tp_1")
VERY_NEGATIVE = -1e30
AUG = 80
PAD = 24
PIECE = 56

F32 = jnp.float32
BF16 = jnp.bfloat16


def axis_index(name):
    return lax.axis_index(name)


def dot(left, right, left_dim, right_dim):
    return lax.dot_general(
        left, right, (((left_dim,), (right_dim,)), ((), ())), preferred_element_type=F32
    )


def split3(value):
    high = value.astype(BF16).astype(F32)
    middle = (value - high).astype(BF16).astype(F32)
    low = (value - high - middle).astype(BF16).astype(F32)
    return high, middle, low


def iota(shape, dim):
    return lax.broadcasted_iota(jnp.int32, shape, dim)


def slot_tables(routes, experts):
    choices, tokens = routes.shape
    expert = iota((experts, tokens), 0)
    named = [(expert == routes[k : k + 1, :]) for k in range(choices)]
    present = named[0]
    for other in named[1:]:
        present = present | other
    before = (iota((tokens, tokens), 0) < iota((tokens, tokens), 1)).astype(F32).astype(BF16)
    slot = dot(present.astype(F32).astype(BF16), before, 1, 0)
    slot_of_row = jnp.concatenate([iota((PAD, tokens), 0)] * experts, axis=0).astype(F32)

    def repeated(table):
        return jnp.concatenate(
            [jnp.broadcast_to(table[e : e + 1, :], (PAD, tokens)) for e in range(experts)], axis=0
        )

    hit = repeated(slot) == slot_of_row
    return [
        jnp.where(hit & (repeated(mask.astype(F32)) > 0.5), 1.0, 0.0).astype(F32) for mask in named
    ]


def first_kernel(q, k, v, gate_in, gate_forget, x, norm_gain, routes, pay, num_out, stat_out):
    segment = q.shape[1]
    blocks = segment // BLK
    head_scale = HEAD ** (-0.5)

    def blocked(ref):
        return jnp.concatenate(
            [ref[0:1, c * BLK : (c + 1) * BLK] for c in range(blocks)], axis=0
        )

    forget = blocked(gate_forget)
    gate = blocked(gate_in)
    small = jnp.exp(-jnp.abs(forget))
    one_more = 1.0 + small
    log1p = jnp.where(one_more == 1.0, small, jnp.log(one_more) * small / (one_more - 1.0 + 1e-38))
    logf = jnp.minimum(forget, 0.0) - log1p
    upper = iota((BLK, BLK), 0) <= iota((BLK, BLK), 1)
    ones_upper = upper.astype(F32).astype(BF16)
    decay = sum(dot(part.astype(BF16), ones_upper, 1, 0) for part in split3(logf))
    ends = decay[:, BLK - 1 : BLK]
    tail = ends - decay + gate
    peaks = jnp.max(tail, axis=1, keepdims=True)
    excess = gate - decay
    excess_columns = jnp.concatenate(
        [excess, jnp.zeros((BLK - blocks, BLK), F32)], axis=0
    ).T
    extra_rows = (iota((AUG - HEAD, BLK), 0) == 0).astype(F32).astype(BF16)

    state = jnp.zeros((AUG, HEAD), F32)
    stable = jnp.full((1, 1), VERY_NEGATIVE, F32)
    passed = jnp.zeros((1, 1), F32)
    for c in range(blocks):
        at = slice(c * BLK, (c + 1) * BLK)
        query, key, value = q[:, at], k[:, at], v[:, at]
        decay_row = decay[c : c + 1, :]
        log_weights = jnp.where(
            upper, excess_columns[:, c : c + 1] + decay_row, VERY_NEGATIVE
        )
        stabilizer = jnp.maximum(
            decay_row + stable, jnp.max(log_weights, axis=0, keepdims=True)
        )
        scores = dot(key, query, 0, 0) * head_scale
        weighted = jnp.exp(log_weights - stabilizer) * scores
        numerator = dot(value, weighted.astype(BF16), 1, 0)
        denominator = jnp.sum(weighted, axis=0, keepdims=True)
        if c:
            high = state.astype(BF16)
            low = (state - high.astype(F32)).astype(BF16)
            carried = dot(high, query, 1, 0) + dot(low, query, 1, 0)
            scale = jnp.exp(decay_row + stable - stabilizer) * head_scale
            numerator = numerator + scale * carried[:HEAD]
            denominator = denominator + scale * carried[HEAD : HEAD + 1]
        num_out[:, at] = numerator
        stat_out[0:1, at] = denominator
        stat_out[1:2, at] = stabilizer
        stat_out[2:3, at] = passed + decay_row
        end = ends[c : c + 1, :]
        following = jnp.maximum(end + stable, peaks[c : c + 1, :])
        key_weight = jnp.exp(tail[c : c + 1, :] - following)
        weighted_keys = (key_weight * key.astype(F32)).astype(BF16)
        update = dot(jnp.concatenate([value, extra_rows], axis=0), weighted_keys, 1, 1)
        state = jnp.exp(end + stable - following) * state + update
        stable = following
        passed = passed + end

    experts = pay.shape[0]
    index = axis_index("tp_0") * lax.axis_size("tp_1") + axis_index("tp_1")
    at = pl.multiple_of(index * BLK, BLK)
    wide = x[...].astype(F32)
    mean = jnp.mean(wide * wide, axis=1, keepdims=True)
    narrow = x[:, pl.ds(at, BLK)].astype(F32) * lax.rsqrt(mean + 1e-06)
    narrow = (narrow * norm_gain[0:1, pl.ds(at, BLK)]).astype(BF16)
    tables = slot_tables(routes[...], experts)
    table = tables[0]
    for other in tables[1:]:
        table = table + other
    slots = dot(table.astype(BF16), narrow, 1, 0)

    lane = iota((1, HEAD), 1)
    scalars = jnp.zeros((1, HEAD), F32)
    for j, part in enumerate(split3(passed) + split3(stable)):
        scalars = jnp.where(lane == j, part, scalars)
    line = jnp.concatenate([state[HEAD : HEAD + 1, :], scalars], axis=1)
    half = HEAD // 2
    packed = jnp.concatenate([state[:half, :], state[half:HEAD, :]], axis=1)
    line_row = iota((PAD, BLK), 0) == PAD - 4
    for e in range(experts):
        rows = jnp.where(line_row, line, slots[e * PAD : (e + 1) * PAD, :])
        pay[e] = jnp.concatenate([rows, packed], axis=0).astype(BF16)


def second_kernel(got, q, num, stat, gain, normed, rows_out, rows):
    peers = got.shape[0]
    segment = q.shape[1]
    head_scale = HEAD ** (-0.5)
    mine = axis_index("ep")
    capacity = rows.shape[0] // peers

    for e in range(peers):
        rows[e * capacity : (e + 1) * capacity, :] = got[e][:capacity].astype(F32)
    packed_rows = rows[...].astype(BF16)
    for i in range(rows_out.shape[0]):
        rows_out[i] = packed_rows

    lines = [got[e, 16:32, :].astype(F32)[PAD - 20 : PAD - 19, :] for e in range(peers)]
    decays = [sum(line[:, HEAD + j : HEAD + j + 1] for j in range(3)) for line in lines]
    levels = [sum(line[:, HEAD + j : HEAD + j + 1] for j in range(3, 6)) for line in lines]
    later = jnp.zeros((1, 1), F32)
    logs = [None] * peers
    for e in reversed(range(peers)):
        earlier = e < mine
        logs[e] = jnp.where(earlier, levels[e] + later, VERY_NEGATIVE)
        later = later + jnp.where(earlier, decays[e], 0.0)
    level = later
    for e in range(peers):
        level = jnp.maximum(level, logs[e])
    half = HEAD // 2
    packed = jnp.zeros((half, BLK), F32)
    line = jnp.zeros((1, BLK), F32)
    for e in range(peers):
        weight = jnp.exp(logs[e] - level)
        packed = packed + weight * got[e].astype(F32)[PAD:PIECE, :]
        line = line + weight * lines[e]
    state = jnp.concatenate(
        [
            packed[:, :HEAD],
            packed[:, HEAD:],
            jnp.where(iota((AUG - HEAD, HEAD), 0) == 0, line[:, :HEAD], 0.0),
        ],
        axis=0,
    )
    high = state.astype(BF16)
    low = (state - high.astype(F32)).astype(BF16)
    square = iota((HEAD, HEAD), 0) == iota((HEAD, HEAD), 1)
    gain_column = jnp.sum(
        jnp.where(square, jnp.broadcast_to(gain[...], (HEAD, HEAD)), 0.0), axis=1, keepdims=True
    )
    width = 2 * BLK
    for c in range(segment // width):
        at = slice(c * width, (c + 1) * width)
        query = q[:, at]
        carried = dot(high, query, 1, 0) + dot(low, query, 1, 0)
        local = stat[1:2, at]
        entering = stat[2:3, at] + level
        stabilizer = jnp.maximum(entering, local)
        scale = jnp.exp(entering - stabilizer) * head_scale
        keep = jnp.exp(local - stabilizer)
        numerator = keep * num[:, at] + scale * carried[:HEAD]
        denominator = keep * stat[0:1, at] + scale * carried[HEAD : HEAD + 1]
        cells = numerator * (1.0 / jnp.maximum(jnp.abs(denominator), jnp.exp(-stabilizer)))
        mean = jnp.mean(cells * cells, axis=0, keepdims=True)
        normed[:, at] = (cells * lax.rsqrt(mean + 1e-06) * gain_column).astype(BF16)


def expert_kernel(own, other, gate, up, down, keep, send):
    slices = own.shape[0]
    width = 2 * BLK
    first = axis_index("tp_1") == 0
    gate_act = None
    for s in range(slices):
        a, b = own[s], other[s]
        left = jnp.concatenate([jnp.where(first, a, b), jnp.where(first, b, a)], axis=1)
        at = slice(s * width, (s + 1) * width)
        gate_part = dot(left, gate[:, at], 1, 1)
        up_part = dot(left, up[:, at], 1, 1)
        gate_act = gate_part if gate_act is None else gate_act + gate_part
        up_act = up_part if s == 0 else up_act + up_part
    hidden = (gate_act / (1.0 + jnp.exp(-gate_act)) * up_act).astype(BF16)
    for s in range(slices):
        piece = dot(hidden, down[:, s * width : (s + 1) * width], 1, 0)
        a, b = piece[:, :BLK], piece[:, BLK:]
        keep[s] = jnp.where(first, a, b).astype(BF16)
        send[s] = jnp.where(first, b, a).astype(BF16)


def sum_kernel(parts, out, rows):
    total = parts[0].astype(F32)
    for s in range(1, parts.shape[0]):
        total = total + parts[s].astype(F32)
    rows[...] = total
    experts, capacity, _ = out.shape
    for e in range(experts):
        out[e] = rows[e * capacity : (e + 1) * capacity, :].astype(BF16)


def last_kernel(got, routes, weight, out):
    experts, capacity, width = got.shape
    tables = slot_tables(routes[...], experts)
    table = None
    for k, one in enumerate(tables):
        part = one * weight[k : k + 1, :]
        table = part if table is None else table + part
    high = table.astype(BF16)
    low = (table - high.astype(F32)).astype(BF16)
    padding = jnp.zeros((PAD - capacity, width), F32)
    pieces = []
    for e in range(experts):
        pieces += [got[e].astype(F32), padding]
    values = jnp.concatenate(pieces, axis=0).astype(BF16)
    out[...] = (dot(high, values, 0, 0) + dot(low, values, 0, 0)).astype(BF16)


def call(kernel, outs, *args, scratch=()):
    return pl.pallas_call(
        kernel,
        out_shape=tuple(jax.ShapeDtypeStruct(*one) for one in outs),
        scratch_shapes=list(scratch),
    )(*args)


def on_device(
    queries,
    key_vectors,
    value_vectors,
    input_gate,
    forget_gate,
    head_gain,
    out_weight,
    expert_input,
    norm_gain,
    routes,
    route_weight,
    gate_weight,
    up_weight,
    down_weight,
):
    segment = queries.shape[0]
    tokens, features = expert_input.shape
    experts = lax.axis_size("ep")
    slices = lax.axis_size("tp_0")
    capacity = 5 * tokens * routes.shape[1] // (4 * experts)
    slots = experts * capacity
    routes_rows = routes.T
    pay, num, stat = call(
        first_kernel,
        [
            ((experts, PIECE, BLK), BF16),
            ((HEAD, segment), F32),
            ((8, segment), F32),
        ],
        queries.T,
        key_vectors.T,
        value_vectors.T,
        input_gate.T,
        forget_gate.T,
        expert_input,
        norm_gain.reshape(1, features),
        routes_rows,
    )
    got = lax.all_to_all(pay, "ep", 0, 0, tiled=True)
    normed, rows = call(
        second_kernel,
        [((HEAD, segment), BF16), ((slices, slots, BLK), BF16)],
        got,
        queries.T,
        num,
        stat,
        head_gain.reshape(1, HEAD),
        scratch=[pltpu.VMEM((slots, BLK), F32)],
    )
    all_normed = lax.all_gather(normed, TP, axis=0, tiled=True)
    swap = [(0, 1), (1, 0)]
    own = lax.all_to_all(rows, "tp_0", 0, 0, tiled=True)
    other = lax.ppermute(own, "tp_1", swap)
    keep, send = call(
        expert_kernel,
        [((slices, slots, BLK), BF16)] * 2,
        own,
        other,
        gate_weight[0].T,
        up_weight[0].T,
        down_weight[0],
    )
    pair = (keep.astype(F32) + lax.ppermute(send, "tp_1", swap).astype(F32)).astype(BF16)
    parts = lax.all_to_all(pair, "tp_0", 0, 0, tiled=True)
    (summed,) = call(
        sum_kernel,
        [((experts, capacity, BLK), BF16)],
        parts,
        scratch=[pltpu.VMEM((slots, BLK), F32)],
    )
    returned = lax.all_to_all(summed, "ep", 0, 0, tiled=True)
    (expert_out,) = call(
        last_kernel, [((tokens, BLK), BF16)], returned, routes_rows, route_weight.T
    )
    mixer_out = dot(all_normed, out_weight, 0, 0).astype(BF16)
    return (mixer_out, expert_out)


def solution(mesh):
    chips = mesh.shape["tp"] // 2
    torus = Mesh(
        mesh.devices.reshape(mesh.shape["grp"], mesh.shape["ep"], chips, 2),
        ("grp", "ep", "tp_0", "tp_1"),
    )
    in_specs = (
        P(("grp", "ep"), TP),
        P(("grp", "ep"), TP),
        P(("grp", "ep"), TP),
        P(("grp", "ep"), TP),
        P(("grp", "ep"), TP),
        P(TP),
        P(None, TP),
        P(("grp", "ep"), None),
        P(),
        P(("grp", "ep"), None),
        P(("grp", "ep"), None),
        P("ep", None, TP),
        P("ep", None, TP),
        P("ep", TP, None),
    )
    out_specs = (P(("grp", "ep"), TP), P(("grp", "ep"), TP))
    return jax.shard_map(
        on_device, mesh=torus, in_specs=in_specs, out_specs=out_specs, check_vma=False
    )
```

time: 247 us -> 182 us (0.74)
  blocking collectives: 58.1 us -> 123 us
  starting transfers between devices: 68.7 us -> 14.3 us
  waiting for transfers between devices: 38.8 us -> 3.86 us
  local copies, waits for them, and re-layouts: 26.6 us -> 0.87 us
  Pallas kernels: 0 us -> 17 us
  other arithmetic: 17.8 us -> 1.28 us
  between operations: 25.4 us -> 14.1 us
  matrix products: 10.7 us -> 4.29 us
    all_to_all x1 -> x4, blocking collectives: 54.8 us -> 123 us  [the longest x1 56.6 us: on_device(): got = lax.all_to_all(pay, 'ep', 0, 0, tiled=True)]
    all_to_all x3 -> x0, starting transfers between devices: 68.4 us -> none  [the longest x1 44.2 us: on_device(): lax.all_to_all(outgoing.reshape(experts, capacity, slice_width), 'ep', sp...]
    all_to_all x3 -> x0, waiting for transfers between devices: 29.1 us -> none  [the longest x1 17.3 us: copy_for_each(): lax.all_to_all(jnp.broadcast_to(shard[None], (peers, *shard.shape)), axis...]
    pallas_call x0 -> x5, Pallas kernels: none -> 17 us  [call(): pl.pallas_call(kernel, out_shape=tuple((jax.ShapeDtypeStruct(*one) for on...]
    ppermute x0 -> x2, starting transfers between devices: none -> 14.3 us  [the longest x1 12 us: on_device(): other = lax.ppermute(own, 'tp_1', swap)]
    slice x49 -> x0, local copies, waits for them, and re-layouts: 10.1 us -> none  [the longest x29 4.17 us: memory_cells(): lax.associative_scan(combine_states, (block_end, matrix_terms, normer_ter...]
    all_gather x2 -> x1, waiting for transfers between devices: 9.53 us -> 0.01 us  [on_device(): all_normed = lax.all_gather(normed, TP, axis=0, tiled=True)]
    dot_general x8 -> x1, matrix products: 10.7 us -> 4.29 us  [dot(): lax.dot_general(left, right, (((left_dim,), (right_dim,)), ((), ())), pre...]
  transfers between devices with their start and end apart: 5 -> 3, of which waited for: 3 -> 2; matrix products, arithmetic and copies ran while one was open for 17% -> 1% of each run, Pallas kernels for 0% -> 5%
where the time goes in v1:
time: 182 us; the launch traced here: 179 us
  blocking collectives  123 us (68%)
  Pallas kernels  17 us (9%)
  starting transfers between devices  14.3 us (8%)
  between operations  14.1 us (8%)
  matrix products  4.29 us (2%)
  waiting for transfers between devices  3.86 us (2%)
    all_to_all x1, blocking collectives, on_device(): got = lax.all_to_all(pay, 'ep', 0, 0, tiled=True)  56.6 us
    all_to_all x1, blocking collectives, on_device(): parts = lax.all_to_all(pair, 'tp_0', 0, 0, tiled=True)  23.9 us
    all_to_all x1, blocking collectives, on_device(): own = lax.all_to_all(rows, 'tp_0', 0, 0, tiled=True)  21.7 us
    all_to_all x1, blocking collectives, on_device(): returned = lax.all_to_all(summed, 'ep', 0, 0, tiled=True)  21.2 us
    pallas_call x5, Pallas kernels, call(): pl.pallas_call(kernel, out_shape=tuple((jax.ShapeDtypeStruct(*one) for on...  17 us
    ppermute x1, starting transfers between devices, on_device(): other = lax.ppermute(own, 'tp_1', swap)  12 us
    dot_general x1, matrix products, dot(): lax.dot_general(left, right, (((left_dim,), (right_dim,)), ((), ())), pre...  4.29 us
  transfers between devices with their start and end apart: 3, of which 2 were waited for; matrix products, arithmetic and copies ran while one was open for 1% of the time, Pallas kernels for 5%

profile of v1, /device:TPU:65, one launch (start us, length us, event | category | flops | bytes accessed | tf_op | source)
XLA Modules:
  0.0 179.1 jit_solution(17133529228855894656)
XLA Ops:
  7.2 0.0 copy-start
  7.2 0.1 all-gather.2.cloned.1.call-start
  7.3 5.5 %shard_map.149 = (bf16[16,56,128]{2,1,0:T(8,128)(2,1)}, f32[64,2048]{1,0:T(8,128)}, f32[8,2048]{1,0:T(8,128)}) custom-call(bf16[64,2048]{1,0:T(8,128)(2,1)} %bitcast.18, bf16[64,2048]{1,0:T(8,128)(2,1)} %bitcast.23, bf16[64,2048]{1,0:T(8,128)(2,1)} %bitcast.24, f32[1,2048]{1,0:T(1,128)} %bitcast.25, f32[1,2048]{1,0:T(1,128)} %bitcast.26, ...), custom_call_target="tpu_custom_call" | custom-call | tf_op jit(solution)/shard_map/pallas_call | solution.py:269
  12.8 56.6 %all_to_all.20.got = bf16[16,56,128]{2,1,0:T(8,128)(2,1)} all-to-all(bf16[16,56,128]{2,1,0:T(8,128)(2,1)} %get-tuple-element.9), channel_id=1, replica_groups=mesh['grp'=2,'ep'=16,'tp_0'=8,'tp_1'=2] {'ep'}, dimensions={0} | all-to-all | bytes 458752 | tf_op jit(solution)/shard_map/all_to_all | solution.py:315
  69.4 3.1 %shard_map.150 = (bf16[64,2048]{1,0:T(8,128)(2,1)}, bf16[8,320,128]{2,1,0:T(8,128)(2,1)}) custom-call(bf16[16,56,128]{2,1,0:T(8,128)(2,1)} %all_to_all.20.got, bf16[64,2048]{1,0:T(8,128)(2,1)} %bitcast.19, f32[64,2048]{1,0:T(8,128)} %get-tuple-element.10.num, f32[8,2048]{1,0:T(8,128)} %get-tuple-element.11.stat, f32[1,64]{1,0:T(1,128)} %bitcast.31), custom_call_target="tpu_custom_call" | custom-call | tf_op jit(solution)/shard_map/pallas_call | solution.py:269
  72.5 0.1 all-gather.2.cloned.1.call-update
  72.6 21.7 %all_to_all.21.own = bf16[8,320,128]{2,1,0:T(8,128)(2,1)S(1)} all-to-all(bf16[8,320,128]{2,1,0:T(8,128)(2,1)} %get-tuple-element.13), channel_id=1, replica_groups=mesh['grp'=2,'ep'=16,'tp_0'=8,'tp_1'=2] {'tp_0'}, dimensions={0} | all-to-all | bytes 1310720 | tf_op jit(solution)/shard_map/all_to_all | solution.py:328
  94.3 0.0 copy-start.1
  94.3 12.0 %collective-permute-start = (bf16[8,320,128]{2,1,0:T(8,128)(2,1)S(1)}, bf16[8,320,128]{2,1,0:T(8,128)(2,1)S(1)}, u32[]{:S(2)}, u32[]{:S(2)}) collective-permute-start(bf16[8,320,128]{2,1,0:T(8,128)(2,1)S(1)} %all_to_all.21.own), channel_id=1, source_target_pairs={{0,1},{1,0},{2,3},{3,2},{4,5},{5,4},{6,7},{7,6},{8,9},{9,8},{10,11... | collective-permute-start | bytes 1966088 | tf_op jit(solution)/shard_map/ppermute | solution.py:329
  106.2 1.8 %collective-permute-done.other = bf16[8,320,128]{2,1,0:T(8,128)(2,1)S(1)} collective-permute-done((bf16[8,320,128]{2,1,0:T(8,128)(2,1)S(1)}, bf16[8,320,128]{2,1,0:T(8,128)(2,1)S(1)}, u32[]{:S(2)}, u32[]{:S(2)}) %collective-permute-start) | collective-permute-done | bytes 655392 | tf_op jit(solution)/shard_map/ppermute | solution.py:329
  108.0 0.0 copy-start.2
  108.0 0.0 copy-done.1
  108.0 0.9 copy-done.2
  108.9 4.6 %shard_map.151 = (bf16[8,320,128]{2,1,0:T(8,128)(2,1)}, bf16[8,320,128]{2,1,0:T(8,128)(2,1)}) custom-call(bf16[8,320,128]{2,1,0:T(8,128)(2,1)} %copy-done.1, bf16[8,320,128]{2,1,0:T(8,128)(2,1)} %copy-done.2, bf16[224,2048]{1,0:T(8,128)(2,1)} %bitcast.20, bf16[224,2048]{1,0:T(8,128)(2,1)} %bitcast.21, bf16[224,2048]{1,0:T(8,128)(2,1)} %bitcast.22), custom_call_target="tpu_custom_call" | custom-call | tf_op jit(solution)/shard_map/pallas_call | solution.py:269
  113.5 2.3 %collective-permute-start.1 = (bf16[8,320,128]{2,1,0:T(8,128)(2,1)}, bf16[8,320,128]{2,1,0:T(8,128)(2,1)S(1)}, u32[]{:S(2)}, u32[]{:S(2)}) collective-permute-start(bf16[8,320,128]{2,1,0:T(8,128)(2,1)} %get-tuple-element.15), channel_id=1, source_target_pairs={{0,1},{1,0},{2,3},{3,2},{4,5},{5,4},{6,7},{7,6},{8,9},{9,8},{10,11... | collective-permute-start | bytes 1966088 | tf_op jit(solution)/shard_map/ppermute | solution.py:339
  115.8 2.0 %collective-permute-done.1 = bf16[8,320,128]{2,1,0:T(8,128)(2,1)S(1)} collective-permute-done((bf16[8,320,128]{2,1,0:T(8,128)(2,1)}, bf16[8,320,128]{2,1,0:T(8,128)(2,1)S(1)}, u32[]{:S(2)}, u32[]{:S(2)}) %collective-permute-start.1) | collective-permute-done | bytes 655392 | tf_op jit(solution)/shard_map/ppermute | solution.py:339
  117.8 1.3 add_convert_fusion
  119.1 23.9 %all_to_all.22.parts = bf16[8,320,128]{2,1,0:T(8,128)(2,1)} all-to-all(bf16[8,320,128]{2,1,0:T(8,128)(2,1)S(1)} %add_convert_fusion), channel_id=1, replica_groups=mesh['grp'=2,'ep'=16,'tp_0'=8,'tp_1'=2] {'tp_0'}, dimensions={0} | all-to-all | bytes 1310720 | tf_op jit(solution)/shard_map/all_to_all | solution.py:340
  142.9 1.8 %shard_map.152 = bf16[16,20,128]{2,1,0:T(8,128)(2,1)} custom-call(bf16[8,320,128]{2,1,0:T(8,128)(2,1)} %all_to_all.22.parts), custom_call_target="tpu_custom_call" | custom-call | tf_op jit(solution)/shard_map/pallas_call | solution.py:269
  144.8 21.2 %all_to_all.23.got = bf16[16,20,128]{2,1,0:T(8,128)(2,1)} all-to-all(bf16[16,20,128]{2,1,0:T(8,128)(2,1)} %shard_map.152), channel_id=1, replica_groups=mesh['grp'=2,'ep'=16,'tp_0'=8,'tp_1'=2] {'ep'}, dimensions={0} | all-to-all | bytes 163840 | tf_op jit(solution)/shard_map/all_to_all | solution.py:347
  166.0 1.9 %shard_map.153 = bf16[128,128]{1,0:T(8,128)(2,1)} custom-call(bf16[16,20,128]{2,1,0:T(8,128)(2,1)} %all_to_all.23.got, s32[2,128]{1,0:T(2,128)} %bitcast.29, f32[2,128]{1,0:T(2,128)} %bitcast.30), custom_call_target="tpu_custom_call" | custom-call | tf_op jit(solution)/shard_map/pallas_call | solution.py:269
  168.0 0.0 all-gather.2.cloned.1.call-done
  168.0 0.0 copy-done
  168.0 4.3 %convolution_convert_fusion = bf16[2048,128]{1,0:T(8,128)(2,1)} fusion(bf16[1024,2048]{1,0:T(8,128)(2,1)} %all-gather.2.cloned.1.call-done, bf16[1024,128]{1,0:T(8,128)(2,1)S(1)} %copy-done), kind=kOutput, calls=%fused_computation | convolution fusion | flops 537133056 | bytes 4980736 | tf_op jit(solution)/shard_map/dot_general | solution.py:28
Async XLA Ops:
  7.2 160.8 %copy-start = (bf16[1024,128]{1,0:T(8,128)(2,1)S(1)}, bf16[1024,128]{1,0:T(8,128)(2,1)}, u32[]{:S(2)}) copy-start(bf16[1024,128]{1,0:T(8,128)(2,1)} %param.20) | copy-start | bytes 786436
  7.2 160.8 %all-gather.2.cloned.1.call-start = ((), (), s32[]{:S(2)}) async-start(), calls=%async_computation.4 | async-start | bytes 4456448 | tf_op jit(solution)/shard_map/all_gather | solution.py:326
  94.3 13.8 %copy-start.1 = (bf16[8,320,128]{2,1,0:T(8,128)(2,1)}, bf16[8,320,128]{2,1,0:T(8,128)(2,1)S(1)}, u32[]{:S(2)}) copy-start(bf16[8,320,128]{2,1,0:T(8,128)(2,1)S(1)} %all_to_all.21.own) | copy-start | bytes 1966084
  94.3 13.8 %collective-permute-start = (bf16[8,320,128]{2,1,0:T(8,128)(2,1)S(1)}, bf16[8,320,128]{2,1,0:T(8,128)(2,1)S(1)}, u32[]{:S(2)}, u32[]{:S(2)}) collective-permute-start(bf16[8,320,128]{2,1,0:T(8,128)(2,1)S(1)} %all_to_all.21.own), channel_id=1, source_target_pairs={{0,1},{1,0},{2,3},{3,2},{4,5},{5,4},{6,7},{7,6},{8,9},{9,8},{10,11... | collective-permute-start | bytes 1966088 | tf_op jit(solution)/shard_map/ppermute | solution.py:329
  108.0 0.9 copy-start.2
  113.5 4.3 %collective-permute-start.1 = (bf16[8,320,128]{2,1,0:T(8,128)(2,1)}, bf16[8,320,128]{2,1,0:T(8,128)(2,1)S(1)}, u32[]{:S(2)}, u32[]{:S(2)}) collective-permute-start(bf16[8,320,128]{2,1,0:T(8,128)(2,1)} %get-tuple-element.15), channel_id=1, source_target_pairs={{0,1},{1,0},{2,3},{3,2},{4,5},{5,4},{6,7},{7,6},{8,9},{9,8},{10,11... | collective-permute-start | bytes 1966088 | tf_op jit(solution)/shard_map/ppermute | solution.py:339
Sparse Core Ops, SparseCore 0:
  72.7 52.1 all-gather.1
